TPU v7x, 32 devices: a whole 2x2x4 slice. The times are simulated.
32 devices in a mesh: sp: 8 (over z, x), tp: 4 (over y, core).
Axes of the slice: x: 2, y: 2, z: 4, core: 2. Of those that a mesh axis runs over, the one named last changes fastest.
Arguments:
- query_small: bfloat16 [6144, 1024], P('sp', 'tp'), may hold values from -18 to 18
- key_small: bfloat16 [6144, 1024], P('sp', 'tp'), may hold values from -6 to 6
- value_small: bfloat16 [6144, 1024], P('sp', 'tp'), may hold values from -6 to 6
- offset_small: bfloat16 [16, 6144], P('tp', 'sp'), may hold values from -25 to 0
- query_large: bfloat16 [6144, 1024], P('sp', 'tp'), may hold values from -18 to 18
- key_large: bfloat16 [6144, 1024], P('sp', 'tp'), may hold values from -6 to 6
- value_large: bfloat16 [6144, 1024], P('sp', 'tp'), may hold values from -6 to 6
- offset_large: bfloat16 [8, 6144], P('tp', 'sp'), may hold values from -25 to 0
- out_small: bfloat16 [1024, 2048], P('tp'), may hold values from -0.125 to 0.125
- out_large: bfloat16 [1024, 2048], P('tp'), may hold values from -0.125 to 0.125
- residual: bfloat16 [6144, 2048], P(('sp', 'tp')), may hold values from -1.1953125 to 1.1953125
- norm_gain: bfloat16 [2048], replicated, may hold values from 0.099609375 to 1.8984375
- gate_weight: bfloat16 [2048, 5632], P('sp', 'tp'), may hold values from -0.125 to 0.125
- up_weight: bfloat16 [2048, 5632], P('sp', 'tp'), may hold values from -0.125 to 0.125
- down_weight: bfloat16 [5632, 2048], P('tp', 'sp'), may hold values from -0.078125 to 0.078125
Outputs:
- layer_out: bfloat16 [6144, 2048], P(('sp', 'tp'))
All inputs are finite; a program needn't handle non-finite values.
Results may differ from a plain program's by a relative error of at most 0.023.
Values may be sent and summed in bfloat16 or wider, within the bound.
A program may use at most 128 MiB of HBM per device.

v0:
```python
import jax
import jax.numpy as jnp
from jax import lax
from jax.sharding import PartitionSpec as P

SMALL_DIM = 64
LARGE_DIM = 128


def split_heads(flat, head_depth):
    return flat.reshape(flat.shape[0], -1, head_depth)


def stick_terms(query, random_keys, values, offset, limits, carried):
    head_depth = query.shape[-1]
    key_heads = split_heads(random_keys, head_depth)
    value_heads = split_heads(values, head_depth)
    logits = jnp.einsum(
        "thd,shd->hts", query, key_heads, preferred_element_type=jnp.float32
    ) * head_depth ** (-0.5)
    logits = logits + offset.astype(jnp.float32)[:, None, :]
    fail_all = jax.nn.log_sigmoid(-logits)
    log_pass = logits + fail_all
    log_fail = fail_all
    before = None
    if limits is not None:
        query_first, key_first = limits
        query_pos = lax.broadcasted_iota(jnp.int32, logits.shape, 1) + query_first
        key_pos = lax.broadcasted_iota(jnp.int32, logits.shape, 2) + key_first
        before = key_pos < query_pos
        log_fail = jnp.where(before, fail_all, 0.0)
    suffix = lax.cumsum(log_fail, axis=2, reverse=True) - log_fail
    weights = jnp.exp(log_pass + suffix + carried[:, :, None])
    if before is not None:
        weights = jnp.where(before, weights, 0.0)
    weights = weights.astype(jnp.bfloat16)
    result = jnp.einsum("hts,shd->thd", weights, value_heads, preferred_element_type=jnp.float32)
    return (result, carried + jnp.sum(log_fail, axis=2))


def both_groups(queries, key_block, limits, totals):
    key_small, value_small, offset_small, key_large, value_large, offset_large = key_block
    out_small, acc_small, out_large, acc_large = totals
    term_small, next_small = stick_terms(
        queries[0], key_small, value_small, offset_small, limits, acc_small
    )
    term_large, next_large = stick_terms(
        queries[1], key_large, value_large, offset_large, limits, acc_large
    )
    return (out_small + term_small, next_small, out_large + term_large, next_large)


def empty_totals(rows, small_heads, large_heads):
    return (
        jnp.zeros((rows, small_heads, SMALL_DIM), jnp.float32),
        jnp.zeros((small_heads, rows), jnp.float32),
        jnp.zeros((rows, large_heads, LARGE_DIM), jnp.float32),
        jnp.zeros((large_heads, rows), jnp.float32),
    )


def rounded(value):
    return lax.optimization_barrier(value.astype(jnp.bfloat16)).astype(jnp.float32)


def rms_norm(stream, gain):
    scale = lax.rsqrt(jnp.mean(stream * stream, axis=-1, keepdims=True) + 1e-06)
    return (stream * scale * gain.astype(jnp.float32)).astype(jnp.bfloat16)


def on_device(
    query_small,
    key_small,
    value_small,
    offset_small,
    query_large,
    key_large,
    value_large,
    offset_large,
    out_small,
    out_large,
    residual,
    norm_gain,
    gate_weight,
    up_weight,
    down_weight,
):
    gate_full, up_full, down_full = (
        lax.all_gather(gate_weight, "sp", axis=0, tiled=True),
        lax.all_gather(up_weight, "sp", axis=0, tiled=True),
        lax.all_gather(down_weight, "sp", axis=1, tiled=True),
    )
    tokens = query_small.shape[0]
    small_heads = offset_small.shape[0]
    large_heads = offset_large.shape[0]
    queries = (split_heads(query_small, SMALL_DIM), split_heads(query_large, LARGE_DIM))
    own_block = (key_small, value_small, offset_small, key_large, value_large, offset_large)
    sp_index = lax.axis_index("sp")
    own_start = sp_index * tokens
    totals = both_groups(
        queries, own_block, (own_start, own_start), empty_totals(tokens, small_heads, large_heads)
    )
    key_dims = (0, 0, 1, 0, 0, 1)
    gathered = (
        lax.all_gather(own_block[0], "sp", axis=0, tiled=True),
        lax.all_gather(own_block[1], "sp", axis=0, tiled=True),
        lax.all_gather(own_block[2], "sp", axis=1, tiled=True),
        lax.all_gather(own_block[3], "sp", axis=0, tiled=True),
        lax.all_gather(own_block[4], "sp", axis=0, tiled=True),
        lax.all_gather(own_block[5], "sp", axis=1, tiled=True),
    )

    def far_turn(turn_index, status):
        first_row = (sp_index - 1 - turn_index) * tokens
        key_block = tuple(
            (
                lax.dynamic_slice_in_dim(member, first_row, tokens, member_dim)
                for member, member_dim in zip(gathered, key_dims)
            )
        )
        return both_groups(queries, key_block, None, status)

    totals = lax.fori_loop(0, sp_index, far_turn, totals)
    mixed_small = totals[0].reshape(tokens, -1).astype(jnp.bfloat16)
    mixed_large = totals[2].reshape(tokens, -1).astype(jnp.bfloat16)
    attended = lax.psum_scatter(
        (
            jnp.dot(mixed_small, out_small, preferred_element_type=jnp.float32)
            + jnp.dot(mixed_large, out_large, preferred_element_type=jnp.float32)
        ).astype(jnp.bfloat16),
        "tp",
        scatter_dimension=0,
        tiled=True,
    ).astype(jnp.float32)
    stream = residual.astype(jnp.float32) + rounded(attended)
    normed = rms_norm(stream, norm_gain)
    normed_rows = lax.all_gather(normed, "tp", axis=0, tiled=True)
    gate = jnp.dot(normed_rows, gate_full, preferred_element_type=jnp.float32)
    upper = jnp.dot(normed_rows, up_full, preferred_element_type=jnp.float32)
    hidden = (jax.nn.silu(gate) * upper).astype(jnp.bfloat16)
    summed = lax.psum_scatter(
        jnp.dot(hidden, down_full, preferred_element_type=jnp.float32).astype(jnp.bfloat16),
        "tp",
        scatter_dimension=0,
        tiled=True,
    ).astype(jnp.float32)
    return (stream + rounded(summed)).astype(jnp.bfloat16)


def solution(mesh):
    return jax.shard_map(
        on_device,
        mesh=mesh,
        in_specs=(
            P("sp", "tp"),
            P("sp", "tp"),
            P("sp", "tp"),
            P("tp", "sp"),
            P("sp", "tp"),
            P("sp", "tp"),
            P("sp", "tp"),
            P("tp", "sp"),
            P("tp", None),
            P("tp", None),
            P(("sp", "tp"), None),
            P(),
            P("sp", "tp"),
            P("sp", "tp"),
            P("tp", "sp"),
        ),
        out_specs=P(("sp", "tp"), None),
        check_vma=False,
    )
```

profile of v0, /device:TPU:0, one launch (start us, length us, event | category | flops | bytes accessed | tf_op | source)
XLA Modules:
  0.0 1540.8 jit_solution(12240522333183597564)
XLA Ops:
  6.5 2.0 copy.45
  8.7 2.0 copy.48
  10.7 1.9 copy.59
  12.7 1.9 copy.60
  15.0 3.1 fusion.36
  18.2 9.5 fusion.45
  27.7 38.7 %fusion.26 = f32[4,768,6,128]{1,2,3,0:T(8,128)} fusion(f32[4,768,6,128]{1,3,2,0:T(8,128)} %bitcast.211), kind=kOutput, calls=%fused_computation.52 | output fusion | flops 299630592 | bytes 18874368 | tf_op jit(solution)/shard_map/reduce-window.4
  67.5 10.0 broadcast_add_fusion.2
  77.7 1.7 fusion.37
  79.5 2.1 copy-done.4
  81.6 6.2 fusion.44
  88.7 11.2 copy.47
  99.9 15.1 fusion.31
  115.0 2.6 copy-done.3
  117.8 3.4 broadcast_add_fusion.3
  122.6 6.4 fusion.33
  130.4 33.4 %all_gather.35 = bf16[2,6144]{1,0:T(2,128)(2,1)} all-gather(bf16[2,768]{1,0:T(2,128)(2,1)S(1)} %copy-done.26), channel_id=1, replica_groups=mesh['sp'=8,'tp'=4] {'sp'}, dimensions={1}, use_global_device_ids=true | all-gather | bytes 27648 | tf_op jit(solution)/shard_map/all_gather | solution.py:110
  163.8 33.6 %all_gather.32 = bf16[4,6144]{1,0:T(4,128)(2,1)} all-gather(bf16[4,768]{1,0:T(4,128)(2,1)S(1)} %copy-done.24), channel_id=1, replica_groups=mesh['sp'=8,'tp'=4] {'sp'}, dimensions={1}, use_global_device_ids=true | all-gather | bytes 55296 | tf_op jit(solution)/shard_map/all_gather | solution.py:107
  197.4 13.6 fusion.28
  212.0 44.0 %all-gather.15.cloned.1.call-done = bf16[6144,256]{0,1:T(8,128)(2,1)} async-done(((bf16[768,256]{0,1:T(8,128)(2,1)}), bf16[6144,256]{0,1:T(8,128)(2,1)}) %all-gather.15.cloned.1.call-update) | async-done | bytes 3145744 | tf_op jit(solution)/shard_map/all_gather | solution.py:108
  256.0 6.2 while.18
  263.6 2.7 add_convert_fusion
  266.9 900.8 %reduce-scatter.3.cloned.1.call-done = bf16[192,2048]{1,0:T(8,128)(2,1)} async-done(((bf16[768,2048]{1,0:T(8,128)(2,1)}), bf16[192,2048]{1,0:T(8,128)(2,1)}) %reduce-scatter.3.cloned.1.call-update) | async-done | bytes 786448 | tf_op jit(solution)/shard_map/reduce_scatter | solution.py:126
  1169.2 2.3 multiply_convert_fusion.1
  1173.0 89.0 %all-gather.19.cloned.1.call-done = bf16[2048,1408]{1,0:T(8,128)(2,1)} async-done(((bf16[256,1408]{1,0:T(8,128)(2,1)}), bf16[2048,1408]{1,0:T(8,128)(2,1)}) %all-gather.19.cloned.1.call-update) | async-done | bytes 5767184 | tf_op jit(solution)/shard_map/all_gather | solution.py:89
  1262.0 28.3 %all-gather.17.cloned.1.call-done = bf16[768,2048]{1,0:T(8,128)(2,1)} async-done(((bf16[192,2048]{1,0:T(8,128)(2,1)}), bf16[768,2048]{1,0:T(8,128)(2,1)}) %all-gather.17.cloned.1.call-update) | async-done | bytes 3145744 | tf_op jit(solution)/shard_map/all_gather | solution.py:137
  1290.3 9.7 fusion.47
  1300.0 84.8 %all-gather.21.cloned.1.call-done = bf16[2048,1408]{1,0:T(8,128)(2,1)} async-done(((bf16[256,1408]{1,0:T(8,128)(2,1)}), bf16[2048,1408]{1,0:T(8,128)(2,1)}) %all-gather.21.cloned.1.call-update) | async-done | bytes 5767184 | tf_op jit(solution)/shard_map/all_gather | solution.py:90
  1384.8 93.4 %all-gather.23.cloned.1.call-done = bf16[1408,2048]{1,0:T(8,128)(2,1)} async-done(((bf16[1408,256]{1,0:T(8,128)(2,1)}), bf16[1408,2048]{1,0:T(8,128)(2,1)}) %all-gather.23.cloned.1.call-update) | async-done | bytes 5767184 | tf_op jit(solution)/shard_map/all_gather | solution.py:91
  1478.2 16.8 %convolution_convert_fusion = bf16[768,2048]{1,0:T(8,128)(2,1)} fusion(bf16[1408,2048]{1,0:T(8,128)(2,1)} %all-gather.23.cloned.1.call-done, f32[768,1408]{1,0:T(8,128)} %fusion.47, bf16[768,2048]{1,0:T(8,128)(2,1)} %all-gather.17.cloned.1.call-done, bf16[2048,1408]{1,0:T(8,128)(2,1)} %all-gather.21.cloned.1.call-done), kind=kOutput, calls=%fused_computation.79 | convolution fusion | flops 8866430976 | bytes 22151168 | tf_op jit(solution)/shard_map/dot_general | solution.py:142
  1495.1 36.2 %reduce-scatter.5.cloned.1.call-done = bf16[192,2048]{1,0:T(8,128)(2,1)} async-done(((bf16[768,2048]{1,0:T(8,128)(2,1)}), bf16[192,2048]{1,0:T(8,128)(2,1)}) %reduce-scatter.5.cloned.1.call-update) | async-done | bytes 786448 | tf_op jit(solution)/shard_map/reduce_scatter | solution.py:141
  1531.3 2.4 add_convert_fusion.1
  (97 shorter events, 11.4 us)
Async XLA Ops:
  6.5 255.8 %copy-start = (bf16[256,2048]{1,0:T(8,128)(2,1)S(1)}, bf16[256,2048]{1,0:T(8,128)(2,1)}, u32[]{:S(2)}) copy-start(bf16[256,2048]{1,0:T(8,128)(2,1)} %param.25) | copy-start | bytes 3145732
  6.5 8.2 copy-start.23
  6.5 8.2 copy-start.14
  6.5 205.4 %all-gather.11.cloned.1.call-start = ((), (), s32[]{:S(2)}) async-start(), calls=%async_computation.3 | async-start | bytes 3538944 | tf_op jit(solution)/shard_map/all_gather | solution.py:105
  8.6 6.4 copy-start.10
  8.6 203.4 %all-gather.9.cloned.1.call-start = ((), (), s32[]{:S(2)}) async-start(), calls=%async_computation.2 | async-start | bytes 3538944 | tf_op jit(solution)/shard_map/all_gather | solution.py:106
  10.7 201.3 %all-gather.13.cloned.1.call-start = ((), (), s32[]{:S(2)}) async-start(), calls=%async_computation.4 | async-start | bytes 3538944 | tf_op jit(solution)/shard_map/all_gather | solution.py:109
  12.7 243.3 %all-gather.15.cloned.1.call-start = ((), (), s32[]{:S(2)}) async-start(), calls=%async_computation.5 | async-start | bytes 3538944 | tf_op jit(solution)/shard_map/all_gather | solution.py:108
  14.7 1153.0 %reduce-scatter.3.cloned.1.call-start = ((), (), s32[]{:S(2)}) async-start(), calls=%async_computation.6 | async-start | bytes 3932160 | tf_op jit(solution)/shard_map/reduce_scatter | solution.py:126
  14.8 3.4 copy-start.21
  14.9 3.2 copy-start.17
  18.1 9.6 copy-start.2
  18.2 9.6 copy-start.8
  67.5 10.1 copy-start.25
  67.5 10.0 copy-start.15
  67.5 10.2 copy-start.16
  87.8 12.1 slice-start.2
  88.7 11.2 slice-start.3
  99.9 22.7 %slice-start.4 = ((s8[4718592]{0:T(1024)(128)(4,1)}), s8[524288]{0:T(1024)(128)(4,1)S(1)}, s32[]{:S(2)}) async-start(s8[4718592]{0:T(1024)(128)(4,1)} %bitcast.216), calls=%async_computation.16 | async-start | bytes 1048576
  117.7 4.8 slice-start.5
  122.6 6.5 copy-start.9
  129.0 34.8 %copy-start.24 = (bf16[4,768]{1,0:T(4,128)(2,1)S(1)}, bf16[4,768]{1,0:T(4,128)(2,1)}, u32[]{:S(2)}) copy-start(bf16[4,768]{1,0:T(4,128)(2,1)} %param.20) | copy-start | bytes 18436
  129.1 68.3 %copy-start.22 = (f32[4,768]{1,0:T(4,128)S(1)}, f32[4,768]{1,0:T(4,128)}, u32[]{:S(2)}) copy-start(f32[4,768]{1,0:T(4,128)} %copy-done.21) | copy-start | bytes 36868
  197.4 13.6 copy-start.7
  263.6 3.3 copy-start.27
  263.6 904.1 %copy-start.5 = (bf16[192,2048]{1,0:T(8,128)(2,1)S(1)}, bf16[192,2048]{1,0:T(8,128)(2,1)}, u32[]{:S(2)}) copy-start(bf16[192,2048]{1,0:T(8,128)(2,1)} %param.27) | copy-start | bytes 2359300
  266.3 995.8 %all-gather.19.cloned.1.call-start = ((), (), s32[]{:S(2)}) async-start(), calls=%async_computation.8 | async-start | bytes 6488064 | tf_op jit(solution)/shard_map/all_gather | solution.py:89
  266.9 1023.5 %all-gather.17.cloned.1.call-start = ((), (), s32[]{:S(2)}) async-start(), calls=%async_computation.7 | async-start | bytes 3932160 | tf_op jit(solution)/shard_map/all_gather | solution.py:137
  1171.5 213.3 %all-gather.21.cloned.1.call-start = ((), (), s32[]{:S(2)}) async-start(), calls=%async_computation.9 | async-start | bytes 6488064 | tf_op jit(solution)/shard_map/all_gather | solution.py:90
  1172.3 306.0 %all-gather.23.cloned.1.call-start = ((), (), s32[]{:S(2)}) async-start(), calls=%async_computation.10 | async-start | bytes 6488064 | tf_op jit(solution)/shard_map/all_gather | solution.py:91
  1173.0 358.3 %reduce-scatter.5.cloned.1.call-start = ((), (), s32[]{:S(2)}) async-start(), calls=%async_computation.11 | async-start | bytes 3932160 | tf_op jit(solution)/shard_map/reduce_scatter | solution.py:141
  1300.0 231.3 %copy-start.6 = (bf16[192,2048]{1,0:T(8,128)(2,1)S(1)}, bf16[192,2048]{1,0:T(8,128)(2,1)}, u32[]{:S(2)}) copy-start(bf16[192,2048]{1,0:T(8,128)(2,1)} %reduce-scatter.3.cloned.1.call-done) | copy-start | bytes 2359300
  (4 other events, 7.3 us)
Sparse Core Ops, SparseCore 0:
  9.6 62.9 all-gather.10
  74.7 58.7 all-gather.8
  135.7 58.8 all-gather.12
  196.7 59.2 all-gather.14
  266.4 901.2 reduce-scatter.2
  1169.7 92.2 all-gather.18
  1263.6 26.6 all-gather.16
  1292.5 92.2 all-gather.20
  1386.9 91.2 all-gather.22
  1495.2 36.0 reduce-scatter.4
where the time goes:
time: 1550 us; the launch traced here: 1540 us
  waiting for transfers between devices  1280 us (83%)
  other arithmetic  109 us (7%)
  blocking collectives  67 us (4%)
  matrix products  37 us (2%)
  local copies, waits for them, and re-layouts  28 us (2%)
    reduce_scatter x1, waiting for transfers between devices, on_device(): lax.psum_scatter((jnp.dot(mixed_small, out_small, preferred_element_type=...  901 us
    all_gather x1, waiting for transfers between devices, on_device(): lax.all_gather(down_weight, 'sp', axis=1, tiled=True)  93.4 us
    all_gather x1, waiting for transfers between devices, on_device(): lax.all_gather(gate_weight, 'sp', axis=0, tiled=True)  89 us
    all_gather x1, waiting for transfers between devices, on_device(): lax.all_gather(up_weight, 'sp', axis=0, tiled=True)  84.8 us
    another operation x4, other arithmetic  54 us
    all_gather x1, waiting for transfers between devices, on_device(): lax.all_gather(own_block[3], 'sp', axis=0, tiled=True)  44 us
    reduce_scatter x1, waiting for transfers between devices, on_device(): lax.psum_scatter(jnp.dot(hidden, down_full, preferred_element_type=jnp.fl...  36.2 us
    all_gather x1, blocking collectives, on_device(): lax.all_gather(own_block[2], 'sp', axis=1, tiled=True)  33.6 us
  transfers between devices with their start and end apart: 10, of which 7 were waited for; matrix products, arithmetic and copies ran while one was open for 9% of the time, Pallas kernels for 0%

commit v1 on v0

v1 whole, which is shorter than its diff:
```python
import math

import jax
import jax.numpy as jnp
from jax import lax
from jax.experimental import pallas as pl
from jax.experimental.pallas import tpu as pltpu
from jax.sharding import PartitionSpec as P


SMALL_DIM = 64
LARGE_DIM = 128
TILE = 256
LANES = 128
LOG2E = math.log2(math.e)


def dot_t(a, b):
    return lax.dot_general(a, b, (((1,), (1,)), ((), ())), preferred_element_type=jnp.float32)


def attend_kernel(
    sp_ref, q_ref, k_small, v_small, k_large, v_large, off_ref, tri_ref, out_ref, qs_ref, acc_ref, carry_ref
):
    tokens = q_ref.shape[0] * pl.num_programs(0)
    small_cols = k_small.shape[1]
    n_small = small_cols // SMALL_DIM
    n_large = k_large.shape[1] // LARGE_DIM
    n_pairs = small_cols // LANES
    lane = lax.broadcasted_iota(jnp.int32, (TILE, LANES), 1)
    low = lane < SMALL_DIM
    zero = jnp.zeros((TILE, LANES), jnp.bfloat16)
    for pair in range(n_pairs):
        q = q_ref[:, pair * LANES : (pair + 1) * LANES]
        qs_ref[2 * pair] = jnp.where(low, q, zero)
        qs_ref[2 * pair + 1] = jnp.where(low, zero, q)
    for head in range(n_large):
        first = small_cols + head * LANES
        qs_ref[n_small + head] = q_ref[:, first : first + LANES]
    acc_ref[...] = jnp.zeros_like(acc_ref)
    carry_ref[...] = jnp.zeros_like(carry_ref)
    tri = tri_ref[...]
    diagonal = sp_ref[0] * (tokens // TILE) + pl.program_id(0)

    def weights_of(head, key, tile, scale, before):
        z = dot_t(qs_ref[head], key) * scale + off_ref[head, tile]
        t = jnp.log(1.0 + jnp.exp2(-jnp.abs(z))) * LOG2E
        log_pass = jnp.minimum(z, 0.0) - t
        log_fail = log_pass - z
        if before is not None:
            log_fail = jnp.where(before, log_fail, 0.0)
        after = jnp.dot(log_fail.astype(jnp.bfloat16), tri, preferred_element_type=jnp.float32)
        carried = carry_ref[head]
        weights = jnp.exp2(log_pass + after + carried)
        if before is not None:
            weights = jnp.where(before, weights, 0.0)
        carry_ref[head] = carried + after[:, :1] + log_fail[:, :1]
        return weights.astype(jnp.bfloat16)

    def one_tile(tile, before):
        rows = pl.ds(pl.multiple_of(tile * TILE, TILE), TILE)
        for pair in range(n_pairs):
            cols = slice(pair * LANES, (pair + 1) * LANES)
            key = k_small[rows, cols]
            value = v_small[rows, cols]
            scale = LOG2E * SMALL_DIM**-0.5
            w0 = weights_of(2 * pair, key, tile, scale, before)
            w1 = weights_of(2 * pair + 1, key, tile, scale, before)
            acc_ref[:, cols] += jnp.dot(
                w0, jnp.where(low, value, zero), preferred_element_type=jnp.float32
            ) + jnp.dot(w1, jnp.where(low, zero, value), preferred_element_type=jnp.float32)
        for head in range(n_large):
            cols = slice(head * LANES, (head + 1) * LANES)
            out_cols = slice(small_cols + head * LANES, small_cols + (head + 1) * LANES)
            w = weights_of(
                n_small + head, k_large[rows, cols], tile, LOG2E * LARGE_DIM**-0.5, before
            )
            acc_ref[:, out_cols] += jnp.dot(
                w, v_large[rows, cols], preferred_element_type=jnp.float32
            )

    row_pos = lax.broadcasted_iota(jnp.int32, (TILE, TILE), 0)
    key_pos = lax.broadcasted_iota(jnp.int32, (TILE, TILE), 1)
    one_tile(diagonal, key_pos < row_pos)

    def step(index, nothing):
        one_tile(diagonal - 1 - index, None)
        return nothing

    lax.fori_loop(0, diagonal, step, 0)
    out_ref[...] = acc_ref[...].astype(jnp.bfloat16)


def attend(sp_index, query, k_small, v_small, k_large, v_large, offsets):
    tokens, cols = query.shape
    heads, length = offsets.shape
    off = (offsets.astype(jnp.float32) * LOG2E).reshape(heads, length // TILE, 1, TILE)
    places = jnp.arange(TILE, dtype=jnp.int32)
    tri = (places[:, None] > places[None, :]).astype(jnp.bfloat16)
    whole = pl.BlockSpec(memory_space=pltpu.VMEM)
    return pl.pallas_call(
        attend_kernel,
        out_shape=jax.ShapeDtypeStruct((tokens, cols), jnp.bfloat16),
        grid=(tokens // TILE,),
        in_specs=[
            pl.BlockSpec(memory_space=pltpu.SMEM),
            pl.BlockSpec((TILE, cols), lambda i: (i, 0)),
            whole,
            whole,
            whole,
            whole,
            whole,
            whole,
        ],
        out_specs=pl.BlockSpec((TILE, cols), lambda i: (i, 0)),
        scratch_shapes=[
            pltpu.VMEM((heads, TILE, LANES), jnp.bfloat16),
            pltpu.VMEM((TILE, cols), jnp.float32),
            pltpu.VMEM((heads, TILE, 1), jnp.float32),
        ],
        compiler_params=pltpu.CompilerParams(vmem_limit_bytes=60 * 1024 * 1024),
        cost_estimate=pl.CostEstimate(
            flops=2 * 3 * heads * tokens * length * TILE,
            bytes_accessed=8 * length * cols,
            transcendentals=3 * heads * tokens * length,
        ),
        name="stick_attend",
    )(sp_index.reshape(1).astype(jnp.int32), query, k_small, v_small, k_large, v_large, off, tri)


def rounded(value):
    return lax.optimization_barrier(value.astype(jnp.bfloat16)).astype(jnp.float32)


def rms_norm(stream, gain):
    scale = lax.rsqrt(jnp.mean(stream * stream, axis=-1, keepdims=True) + 1e-06)
    return (stream * scale * gain.astype(jnp.float32)).astype(jnp.bfloat16)


def layer(
    query_small,
    key_small,
    value_small,
    offset_small,
    query_large,
    key_large,
    value_large,
    offset_large,
    out_small,
    out_large,
    residual,
    norm_gain,
    gate_weight,
    up_weight,
    down_weight,
):
    sp_index = lax.axis_index("sp")
    members = tuple(
        lax.all_gather(member, "sp", axis=0, tiled=True)
        for member in (key_small, value_small, key_large, value_large)
    )
    offsets = lax.all_gather(
        jnp.concatenate([offset_small, offset_large], axis=0), "sp", axis=1, tiled=True
    )
    members, offsets, gate_weight, up_weight, down_weight = lax.optimization_barrier(
        (members, offsets, gate_weight, up_weight, down_weight)
    )
    gate_full = lax.all_gather(gate_weight, "sp", axis=0, tiled=True)
    up_full = lax.all_gather(up_weight, "sp", axis=0, tiled=True)
    down_full = lax.all_gather(down_weight, "sp", axis=1, tiled=True)
    query = jnp.concatenate([query_small, query_large], axis=1)
    out_rows = jnp.concatenate([out_small, out_large], axis=0)
    mixed = attend(sp_index, query, *members, offsets)
    attended = lax.psum_scatter(
        jnp.dot(mixed, out_rows, preferred_element_type=jnp.float32).astype(jnp.bfloat16),
        "tp",
        scatter_dimension=0,
        tiled=True,
    ).astype(jnp.float32)
    stream = residual.astype(jnp.float32) + rounded(attended)
    normed = rms_norm(stream, norm_gain)
    normed_rows = lax.all_gather(normed, "tp", axis=0, tiled=True)
    gate = jnp.dot(normed_rows, gate_full, preferred_element_type=jnp.float32)
    upper = jnp.dot(normed_rows, up_full, preferred_element_type=jnp.float32)
    hidden = (jax.nn.silu(gate) * upper).astype(jnp.bfloat16)
    summed = lax.psum_scatter(
        jnp.dot(hidden, down_full, preferred_element_type=jnp.float32).astype(jnp.bfloat16),
        "tp",
        scatter_dimension=0,
        tiled=True,
    ).astype(jnp.float32)
    return (stream + rounded(summed)).astype(jnp.bfloat16)


def solution(mesh):
    return jax.shard_map(
        layer,
        mesh=mesh,
        in_specs=(
            P("sp", "tp"),
            P("sp", "tp"),
            P("sp", "tp"),
            P("tp", "sp"),
            P("sp", "tp"),
            P("sp", "tp"),
            P("sp", "tp"),
            P("tp", "sp"),
            P("tp", None),
            P("tp", None),
            P(("sp", "tp"), None),
            P(),
            P("sp", "tp"),
            P("sp", "tp"),
            P("tp", "sp"),
        ),
        out_specs=P(("sp", "tp"), None),
        check_vma=False,
    )
```

time: 1550 us -> 797 us (0.51)
  waiting for transfers between devices: 1280 us -> 693 us
  other arithmetic: 109 us -> 9.65 us
  blocking collectives: 67 us -> 32.7 us
  local copies, waits for them, and re-layouts: 28 us -> 0.9 us
  Pallas kernels: 0 us -> 16.1 us
    reduce_scatter x2, waiting for transfers between devices: 937 us -> 183 us  [the longest x1 147 us: layer(): lax.psum_scatter(jnp.dot(mixed, out_rows, preferred_element_type=jnp.floa...]
    all_gather x8, waiting for transfers between devices: 340 us -> 505 us  [the longest x4 210 us: layer(): lax.all_gather(member, 'sp', axis=0, tiled=True)]
    another operation x6 -> x0, other arithmetic: 67.4 us -> none
    all_gather x2 -> x1, blocking collectives: 67 us -> 32.7 us  [layer(): lax.all_gather(jnp.concatenate([offset_small, offset_large], axis=0), 'sp...]
    convert_element_type x7 -> x2, other arithmetic: 22.5 us -> 3.06 us  [the longest x1 2.4 us: layer(): return (stream + rounded(summed)).astype(jnp.bfloat16)]
    pallas_call x0 -> x1, Pallas kernels: none -> 16.1 us  [attend(): pl.pallas_call(attend_kernel, out_shape=jax.ShapeDtypeStruct((tokens, col...]
    reduce_sum x2 -> x0, other arithmetic: 15.7 us -> none  [stick_terms(): return (result, carried + jnp.sum(log_fail, axis=2))]
    dot_general x8 -> x3, matrix products: 37 us -> 31.1 us  [the longest x1 16.8 us: layer(): jnp.dot(hidden, down_full, preferred_element_type=jnp.float32)]
  transfers between devices with their start and end apart: 10 -> 10, of which waited for: 7 -> 10; matrix products, arithmetic and copies ran while one was open for 9% -> 2% of each run, Pallas kernels for 0% -> 0%
where the time goes in v1:
time: 797 us
  waiting for transfers between devices  693 us (87%)
  blocking collectives  32.7 us (4%)
  matrix products  31.1 us (4%)
  Pallas kernels  16.1 us (2%)
  between operations  13.6 us (2%)
  other arithmetic  9.65 us (1%)
    all_gather x4, waiting for transfers between devices, layer(): lax.all_gather(member, 'sp', axis=0, tiled=True)  210 us
    reduce_scatter x1, waiting for transfers between devices, layer(): lax.psum_scatter(jnp.dot(mixed, out_rows, preferred_element_type=jnp.floa...  147 us
    all_gather x1, waiting for transfers between devices, layer(): down_full = lax.all_gather(down_weight, 'sp', axis=1, tiled=True)  93.4 us
    all_gather x1, waiting for transfers between devices, layer(): gate_full = lax.all_gather(gate_weight, 'sp', axis=0, tiled=True)  89 us
    all_gather x1, waiting for transfers between devices, layer(): up_full = lax.all_gather(up_weight, 'sp', axis=0, tiled=True)  84.8 us
    reduce_scatter x1, waiting for transfers between devices, layer(): lax.psum_scatter(jnp.dot(hidden, down_full, preferred_element_type=jnp.fl...  36.2 us
    all_gather x1, blocking collectives, layer(): lax.all_gather(jnp.concatenate([offset_small, offset_large], axis=0), 'sp...  32.7 us
    all_gather x1, waiting for transfers between devices, layer(): normed_rows = lax.all_gather(normed, 'tp', axis=0, tiled=True)  28.3 us
  transfers between devices with their start and end apart: 10, of which 10 were waited for; matrix products, arithmetic and copies ran while one was open for 2% of the time, Pallas kernels for 0%

profile of v1, /device:TPU:0, one launch (start us, length us, event | category | flops | bytes accessed | tf_op | source)
XLA Modules:
  0.0 796.9 jit_solution(163287446664276297)
XLA Ops:
  6.5 0.7 all-gather.11.cloned.1.call-update
  7.3 0.7 all-gather.13.cloned.1.call-update
  8.1 0.7 all-gather.15.cloned.1.call-update
  8.8 0.5 all-gather.9.cloned.1.call-update
  9.3 0.0 reduce-scatter.3.cloned.1.call-start
  9.4 0.7 pad_maximum_fusion.1
  10.1 32.7 %all_gather.31 = bf16[6,6144]{1,0:T(8,128)(2,1)S(1)} all-gather(bf16[6,768]{1,0:T(8,128)(2,1)S(1)} %pad_maximum_fusion.1), channel_id=1, replica_groups=mesh['sp'=8,'tp'=4] {'sp'}, dimensions={1}, use_global_device_ids=true | all-gather | bytes 82944 | tf_op jit(solution)/shard_map/all_gather | solution.py:162
  42.7 0.7 fusion.3.tri_ref
  43.4 2.0 pad_maximum_fusion.q_ref
  45.4 27.2 %all-gather.11.cloned.1.call-done.v_small = bf16[6144,256]{1,0:T(8,128)(2,1)} async-done(((bf16[768,256]{1,0:T(8,128)(2,1)}), bf16[6144,256]{1,0:T(8,128)(2,1)}) %all-gather.11.cloned.1.call-update) | async-done | bytes 3145744 | tf_op jit(solution)/shard_map/all_gather | solution.py:159
  72.6 60.9 %all-gather.13.cloned.1.call-done.k_large = bf16[6144,256]{1,0:T(8,128)(2,1)} async-done(((bf16[768,256]{1,0:T(8,128)(2,1)}), bf16[6144,256]{1,0:T(8,128)(2,1)}) %all-gather.13.cloned.1.call-update) | async-done | bytes 3145744 | tf_op jit(solution)/shard_map/all_gather | solution.py:159
  133.5 60.9 %all-gather.15.cloned.1.call-done.v_large = bf16[6144,256]{1,0:T(8,128)(2,1)} async-done(((bf16[768,256]{1,0:T(8,128)(2,1)}), bf16[6144,256]{1,0:T(8,128)(2,1)}) %all-gather.15.cloned.1.call-update) | async-done | bytes 3145744 | tf_op jit(solution)/shard_map/all_gather | solution.py:159
  194.4 60.7 %all-gather.9.cloned.1.call-done.k_small = bf16[6144,256]{1,0:T(8,128)(2,1)} async-done(((bf16[768,256]{1,0:T(8,128)(2,1)}), bf16[6144,256]{1,0:T(8,128)(2,1)}) %all-gather.9.cloned.1.call-update) | async-done | bytes 3145744 | tf_op jit(solution)/shard_map/all_gather | solution.py:159
  255.2 0.9 reshape.16.off_ref
  256.0 16.1 %stick_attend.1 = bf16[768,512]{1,0:T(8,128)(2,1)} custom-call(s32[1]{0:T(128)} %bitcast.sp_ref, bf16[768,512]{1,0:T(8,128)(2,1)} %pad_maximum_fusion.q_ref, bf16[6144,256]{1,0:T(8,128)(2,1)} %all-gather.9.cloned.1.call-done.k_small, bf16[6144,256]{1,0:T(8,128)(2,1)} %all-gather.11.cloned.1.call-done.v_small, ...), custom_call_target="tpu_custom_call" | custom-call | flops 43486543872 | bytes 25165824 | tf_op jit(solution)/shard_map/stick_attend/pallas_call | solution.py:101
  272.1 4.6 convolution_convert_fusion
  276.7 0.0 all-gather.19.cloned.1.call-start
  276.8 0.5 all-gather.19.cloned.1.call-update
  277.4 146.6 %reduce-scatter.3.cloned.1.call-done = bf16[192,2048]{1,0:T(8,128)(2,1)} async-done(((bf16[768,2048]{1,0:T(8,128)(2,1)}), bf16[192,2048]{1,0:T(8,128)(2,1)}) %reduce-scatter.3.cloned.1.call-update) | async-done | bytes 786448 | tf_op jit(solution)/shard_map/reduce_scatter | solution.py:174
  424.0 1.5 multiply_reduce_fusion
  425.5 2.3 multiply_convert_fusion.1
  427.9 0.0 all-gather.21.cloned.1.call-start
  427.9 0.7 all-gather.21.cloned.1.call-update
  428.7 0.7 all-gather.23.cloned.1.call-update
  429.4 89.0 %all-gather.19.cloned.1.call-done = bf16[2048,1408]{1,0:T(8,128)(2,1)} async-done(((bf16[256,1408]{1,0:T(8,128)(2,1)}), bf16[2048,1408]{1,0:T(8,128)(2,1)}) %all-gather.19.cloned.1.call-update) | async-done | bytes 5767184 | tf_op jit(solution)/shard_map/all_gather | solution.py:168
  518.4 28.3 %all-gather.17.cloned.1.call-done = bf16[768,2048]{1,0:T(8,128)(2,1)} async-done(((bf16[192,2048]{1,0:T(8,128)(2,1)}), bf16[768,2048]{1,0:T(8,128)(2,1)}) %all-gather.17.cloned.1.call-update) | async-done | bytes 3145744 | tf_op jit(solution)/shard_map/all_gather | solution.py:182
  546.7 9.7 %fusion.6 = f32[768,1408]{1,0:T(8,128)} fusion(bf16[768,2048]{1,0:T(8,128)(2,1)} %all-gather.17.cloned.1.call-done, bf16[2048,1408]{1,0:T(8,128)(2,1)} %all-gather.19.cloned.1.call-done), kind=kOutput, calls=%fused_computation.18 | convolution fusion | flops 4429185024 | bytes 13238272 | tf_op jit(solution)/shard_map/dot_general | solution.py:183
  556.4 84.8 %all-gather.21.cloned.1.call-done = bf16[2048,1408]{1,0:T(8,128)(2,1)} async-done(((bf16[256,1408]{1,0:T(8,128)(2,1)}), bf16[2048,1408]{1,0:T(8,128)(2,1)}) %all-gather.21.cloned.1.call-update) | async-done | bytes 5767184 | tf_op jit(solution)/shard_map/all_gather | solution.py:169
  641.2 93.4 %all-gather.23.cloned.1.call-done = bf16[1408,2048]{1,0:T(8,128)(2,1)} async-done(((bf16[1408,256]{1,0:T(8,128)(2,1)}), bf16[1408,2048]{1,0:T(8,128)(2,1)}) %all-gather.23.cloned.1.call-update) | async-done | bytes 5767184 | tf_op jit(solution)/shard_map/all_gather | solution.py:170
  734.6 16.8 %convolution_convert_fusion.1 = bf16[768,2048]{1,0:T(8,128)(2,1)} fusion(bf16[1408,2048]{1,0:T(8,128)(2,1)} %all-gather.23.cloned.1.call-done, f32[768,1408]{1,0:T(8,128)} %fusion.6, bf16[768,2048]{1,0:T(8,128)(2,1)} %all-gather.17.cloned.1.call-done, bf16[2048,1408]{1,0:T(8,128)(2,1)} %all-gather.21.cloned.1.call-done), kind=kOutput, calls=%fused_computation.2 | convolution fusion | flops 8866430976 | bytes 22151168 | tf_op jit(solution)/shard_map/dot_general | solution.py:187
  751.4 36.2 %reduce-scatter.5.cloned.1.call-done = bf16[192,2048]{1,0:T(8,128)(2,1)} async-done(((bf16[768,2048]{1,0:T(8,128)(2,1)}), bf16[192,2048]{1,0:T(8,128)(2,1)}) %reduce-scatter.5.cloned.1.call-update) | async-done | bytes 786448 | tf_op jit(solution)/shard_map/reduce_scatter | solution.py:186
  787.6 2.4 add_convert_fusion
  (23 shorter events, 0.4 us)
Async XLA Ops:
  6.5 66.1 %all-gather.11.cloned.1.call-start = ((), (), s32[]{:S(2)}) async-start(), calls=%async_computation.3 | async-start | bytes 3538944 | tf_op jit(solution)/shard_map/all_gather | solution.py:159
  7.3 126.2 %all-gather.13.cloned.1.call-start = ((), (), s32[]{:S(2)}) async-start(), calls=%async_computation.4 | async-start | bytes 3538944 | tf_op jit(solution)/shard_map/all_gather | solution.py:159
  8.0 186.4 %all-gather.15.cloned.1.call-start = ((), (), s32[]{:S(2)}) async-start(), calls=%async_computation.5 | async-start | bytes 3538944 | tf_op jit(solution)/shard_map/all_gather | solution.py:159
  8.7 246.4 %all-gather.9.cloned.1.call-start = ((), (), s32[]{:S(2)}) async-start(), calls=%async_computation.2 | async-start | bytes 3538944 | tf_op jit(solution)/shard_map/all_gather | solution.py:159
  9.3 414.7 %reduce-scatter.3.cloned.1.call-start = ((), (), s32[]{:S(2)}) async-start(), calls=%async_computation.6 | async-start | bytes 3932160 | tf_op jit(solution)/shard_map/reduce_scatter | solution.py:174
  256.0 16.1 %copy-start.3 = (bf16[256,2048]{1,0:T(8,128)(2,1)S(1)}, bf16[256,2048]{1,0:T(8,128)(2,1)}, u32[]{:S(2)}) copy-start(bf16[256,2048]{1,0:T(8,128)(2,1)} %param.24) | copy-start | bytes 3145732
  256.0 16.1 %copy-start.4 = (bf16[256,2048]{1,0:T(8,128)(2,1)S(1)}, bf16[256,2048]{1,0:T(8,128)(2,1)}, u32[]{:S(2)}) copy-start(bf16[256,2048]{1,0:T(8,128)(2,1)} %param.23) | copy-start | bytes 3145732
  276.7 0.7 copy-start.2
  276.7 147.3 %copy-start = (bf16[192,2048]{1,0:T(8,128)(2,1)S(1)}, bf16[192,2048]{1,0:T(8,128)(2,1)}, u32[]{:S(2)}) copy-start(bf16[192,2048]{1,0:T(8,128)(2,1)} %param.25) | copy-start | bytes 2359300
  276.7 241.7 %all-gather.19.cloned.1.call-start = ((), (), s32[]{:S(2)}) async-start(), calls=%async_computation.8 | async-start | bytes 6488064 | tf_op jit(solution)/shard_map/all_gather | solution.py:168
  277.3 269.4 %all-gather.17.cloned.1.call-start = ((), (), s32[]{:S(2)}) async-start(), calls=%async_computation.7 | async-start | bytes 3932160 | tf_op jit(solution)/shard_map/all_gather | solution.py:182
  427.9 213.4 %all-gather.21.cloned.1.call-start = ((), (), s32[]{:S(2)}) async-start(), calls=%async_computation.9 | async-start | bytes 6488064 | tf_op jit(solution)/shard_map/all_gather | solution.py:169
  428.6 306.0 %all-gather.23.cloned.1.call-start = ((), (), s32[]{:S(2)}) async-start(), calls=%async_computation.10 | async-start | bytes 6488064 | tf_op jit(solution)/shard_map/all_gather | solution.py:170
  429.3 358.3 %reduce-scatter.5.cloned.1.call-start = ((), (), s32[]{:S(2)}) async-start(), calls=%async_computation.11 | async-start | bytes 3932160 | tf_op jit(solution)/shard_map/reduce_scatter | solution.py:186
  751.4 36.2 %copy-start.1 = (bf16[192,2048]{1,0:T(8,128)(2,1)S(1)}, bf16[192,2048]{1,0:T(8,128)(2,1)}, u32[]{:S(2)}) copy-start(bf16[192,2048]{1,0:T(8,128)(2,1)} %reduce-scatter.3.cloned.1.call-done) | copy-start | bytes 2359300
Sparse Core Ops, SparseCore 0:
  9.5 63.0 all-gather.10
  74.8 58.6 all-gather.12
  135.7 58.6 all-gather.14
  196.4 58.6 all-gather.8
  276.9 147.1 reduce-scatter.2
  426.1 92.2 all-gather.18
  520.0 26.6 all-gather.16
  548.9 92.2 all-gather.20
  643.3 91.2 all-gather.22
  751.5 36.0 reduce-scatter.4
